TPU v7x, 128 devices: a whole 4x4x4 slice. The times are simulated.
128 devices in a mesh: sp: 32 (over z, y, core), tp: 4 (over x).
Axes of the slice: x: 4, y: 4, z: 4, core: 2. Of those that a mesh axis runs over, the one named last changes fastest.
Arguments:
- query_rows: bfloat16 [32768, 1024], P('sp', 'tp'), may hold values from -6 to 6
- key_rows: bfloat16 [32768, 1024], P('sp', 'tp'), may hold values from -6 to 6
- value_rows: bfloat16 [32768, 1024], P('sp', 'tp'), may hold values from -6 to 6
- input_gate: float32 [8, 32768], P('tp', 'sp'), may hold values from -4 to 255
- forget_gate: float32 [8, 32768], P('tp', 'sp'), may hold values from -3 to 20
- output_gate: bfloat16 [32768, 1024], P('sp', 'tp'), may hold values from -6 to 6
- documents: int32 [32768], P('sp'), may hold values from 0 to 7, never falling along the last dimension, each value on 1 to 6144 neighbouring positions
- residual: bfloat16 [32768, 2048], P(('sp', 'tp')), may hold values from -6 to 6
- out_weight: bfloat16 [1024, 2048], P('tp'), may hold values from -0.375 to 0.375
- norm_gain: bfloat16 [2048], replicated, may hold values from 0.099609375 to 1.8984375
- gate_weight: bfloat16 [2048, 5632], P('sp', 'tp'), may hold values from -0.125 to 0.125
- up_weight: bfloat16 [2048, 5632], P('sp', 'tp'), may hold values from -0.125 to 0.125
- down_weight: bfloat16 [5632, 2048], P('tp', 'sp'), may hold values from -0.15625 to 0.15625
Outputs:
- layer_out: bfloat16 [32768, 2048], P(('sp', 'tp'))
Inputs may be any that keep to these rules, and one draw needn't show every extreme that they name: `documents`: document numbers never fall along the positions; each document covers 1 to 6144 positions and one covers exactly 6144.
All inputs are finite; a program needn't handle non-finite values.
Results may differ from a plain program's by a relative error of at most 0.013.
Values may be sent and summed in bfloat16 or wider, within the bound.
A program may use at most 128 MiB of HBM per device.

v0:
```python
import jax
import jax.numpy as jnp
from jax import lax
from jax.sharding import Mesh
from jax.sharding import PartitionSpec as P

HD = 128
BLOCK = 128
SP = ("sp_0", "sp_1", "sp_2")
SP_TP = ("sp_0", "sp_1", "sp_2", "tp")
neg_large = -1e30
norm_eps = 1e-06
highest = lax.Precision.HIGHEST


def gather_turned(arrays, axis, dims):
    turned = [jnp.moveaxis(a, dim, 0) for a, dim in zip(arrays, dims)]
    both = jnp.concatenate([t.reshape(len(t), -1) for t in turned], axis=1)
    whole, at, finished = (lax.all_gather(both, axis, axis=0, tiled=True), 0, [])
    for t, dim in zip(turned, dims):
        slab = whole[:, at : at + t[0].size].reshape(-1, *t.shape[1:])
        finished.append(jnp.moveaxis(slab, 0, dim))
        at += t[0].size
    return tuple(finished)


def nothing_yet(array, identity):
    return jax.tree.map(
        lambda part, zero: jnp.zeros_like(part) + jnp.asarray(zero, part.dtype), array, identity
    )


def all_in_one(array, axis):
    leaves = jax.tree.leaves(array)
    sequence = sorted(range(len(leaves)), key=lambda k: -leaves[k].size)
    width = (1, *leaves[sequence[0]].shape)[-1]
    lines = [
        jnp.pad(leaves[k].reshape(-1), (0, -leaves[k].size % width)).reshape(-1, width)
        for k in sequence
    ]
    both, at, found = (lax.all_gather(jnp.concatenate(lines), axis), 0, {})
    for k, line in zip(sequence, lines):
        slab = both[:, at : at + len(line)].reshape(len(both), -1)
        found[k] = slab[:, : leaves[k].size].reshape(-1, *leaves[k].shape)
        at += len(line)
    numbers = iter(range(len(leaves)))
    return jax.tree.map(lambda _: found[next(numbers)], array)


def gathered_by_type(array, axis):
    leaves, found = (jax.tree.leaves(array), {})
    for leading, a in enumerate(leaves):
        if leading not in found:
            alike = [k for k, b in enumerate(leaves) if b.dtype == a.dtype]
            got = (
                all_in_one([leaves[k] for k in alike], axis)
                if len(alike) > 1
                else [lax.all_gather(a, axis)]
            )
            for k, b in zip(alike, got):
                found[k] = b
    numbers = iter(range(len(leaves)))
    return jax.tree.map(lambda _: found[next(numbers)], array)


def prefix_by_axis(array, axes, combine, identity):
    before = start = nothing_yet(array, identity)
    total = array
    for axis in reversed(axes):
        devices, position = (lax.axis_size(axis), lax.axis_index(axis))
        pieces = gathered_by_type(total, axis)
        inside, total = (start, start)
        for k in range(devices):
            passed = k < position
            total = combine(total, jax.tree.map(lambda part: part[k], pieces))
            inside = jax.tree.map(lambda new, old: jnp.where(passed, new, old), total, inside)
        before = combine(inside, before)
    return before


def block_step(carried, inputs):
    memory, normer, stab_prev, carry_doc = carried
    queries, key_float, value_float, gate_in, log_forget, docs = inputs
    cumlog = jnp.cumsum(log_forget, axis=1)
    length = docs.shape[0]
    target_positions = jnp.arange(length)
    same_doc = (docs[:, None] == docs[None, :]) & (
        target_positions[:, None] >= target_positions[None, :]
    )
    log_weight = jnp.where(
        same_doc[None], cumlog[:, :, None] - cumlog[:, None, :] + gate_in[:, None, :], neg_large
    )
    carried_log = jnp.where((docs == carry_doc)[None, :], cumlog + stab_prev[:, None], neg_large)
    stabilizer = jnp.maximum(carried_log, jnp.max(log_weight, axis=2))
    scores = jnp.einsum("lhd,shd->hls", queries, key_float, precision=highest)
    weighted = scores * jnp.exp(log_weight - stabilizer[:, :, None])
    carried_scale = jnp.exp(carried_log - stabilizer)
    numerator = carried_scale[:, :, None] * jnp.einsum(
        "lhd,hde->hle", queries, memory, precision=highest
    )
    numerator = numerator + jnp.einsum("hls,she->hle", weighted, value_float, precision=highest)
    denominator = carried_scale * jnp.einsum(
        "lhd,hd->hl", queries, normer, precision=highest
    ) + jnp.sum(weighted, axis=2)
    outputs = numerator / jnp.maximum(jnp.abs(denominator), 1.0)[:, :, None]
    last_doc = docs[-1]
    inject_log = jnp.where(
        (docs == last_doc)[None, :], cumlog[:, -1:] - cumlog + gate_in, neg_large
    )
    inject_max = jnp.max(inject_log, axis=1)
    weights = jnp.exp(inject_log - inject_max[:, None])
    continues = carry_doc == last_doc
    stab_new = jnp.where(continues, jnp.maximum(cumlog[:, -1] + stab_prev, inject_max), inject_max)
    decay_scale = jnp.where(continues, jnp.exp(cumlog[:, -1] + stab_prev - stab_new), 0.0)
    inject = jnp.exp(inject_max - stab_new)
    memory_step = jnp.einsum(
        "lhd,lhe->hde", key_float * weights.T[:, :, None], value_float, precision=highest
    )
    normer_step = jnp.einsum("hl,lhd->hd", weights, key_float, precision=highest)
    memory = decay_scale[:, None, None] * memory + inject[:, None, None] * memory_step
    normer = decay_scale[:, None] * normer + inject[:, None] * normer_step
    return ((memory, normer, stab_new, last_doc), jnp.transpose(outputs, (1, 0, 2)))


def run_blocks(queries, key_float, value_float, gate_in, log_forget, docs, start_state):
    length, heads, width = queries.shape
    count = length // BLOCK
    inputs = (
        queries.reshape(count, BLOCK, heads, width),
        key_float.reshape(count, BLOCK, heads, width),
        value_float.reshape(count, BLOCK, heads, width),
        jnp.moveaxis(gate_in.reshape(heads, count, BLOCK), 1, 0),
        jnp.moveaxis(log_forget.reshape(heads, count, BLOCK), 1, 0),
        docs.reshape(count, BLOCK),
    )
    final, outputs = lax.scan(block_step, start_state, inputs)
    return (outputs.reshape(length, heads, width), final)


def join_states(earlier, later_part):
    memory_early, normer_early, stab_early, total_early, doc_early = earlier
    memory_late, normer_late, stab_late, total_late, doc_late = later_part
    continues = doc_late == doc_early
    is_empty = doc_late < 0
    stab_both = jnp.where(continues, jnp.maximum(total_late + stab_early, stab_late), stab_late)
    scale_early = jnp.where(continues, jnp.exp(total_late + stab_early - stab_both), 0.0)
    scale_late = jnp.exp(stab_late - stab_both)
    memory = scale_early[:, None, None] * memory_early + scale_late[:, None, None] * memory_late
    normer = scale_early[:, None] * normer_early + scale_late[:, None] * normer_late
    return (
        jnp.where(is_empty, memory_early, memory),
        jnp.where(is_empty, normer_early, normer),
        jnp.where(is_empty, stab_early, stab_both),
        total_early + total_late,
        jnp.where(is_empty, doc_early, doc_late),
    )


def body(
    query_rows,
    key_rows,
    value_rows,
    input_gate,
    forget_gate,
    output_gate,
    documents,
    residual,
    out_weight,
    norm_gain,
    gate_weight,
    up_weight,
    down_weight,
):
    whole_gate, whole_up, whole_down = gather_turned(
        (gate_weight, up_weight, down_weight), SP, (0, 0, 1)
    )
    tokens = query_rows.shape[0]
    local_heads = input_gate.shape[0]
    queries = query_rows.astype(jnp.float32).reshape(tokens, local_heads, HD) * HD ** (-0.5)
    key_float = key_rows.astype(jnp.float32).reshape(tokens, local_heads, HD)
    value_float = value_rows.astype(jnp.float32).reshape(tokens, local_heads, HD)
    log_forget = jax.nn.log_sigmoid(forget_gate)
    cumlog = jnp.cumsum(log_forget, axis=1)
    total = cumlog[:, -1]
    last_doc = documents[-1]
    inject_log = jnp.where(
        (documents == last_doc)[None, :], total[:, None] - cumlog + input_gate, neg_large
    )
    inject_max = jnp.max(inject_log, axis=1)
    weights = jnp.exp(inject_log - inject_max[:, None])
    memory = jnp.einsum(
        "thd,the->hde", key_float * weights.T[:, :, None], value_float, precision=highest
    )
    normer = jnp.einsum("ht,thd->hd", weights, key_float, precision=highest)
    identity = (
        jnp.zeros_like(memory),
        jnp.zeros_like(normer),
        jnp.full_like(inject_max, neg_large),
        jnp.zeros_like(total),
        jnp.array(-1, jnp.int32),
    )
    before = prefix_by_axis(
        (memory, normer, inject_max, total, last_doc), SP, join_states, identity
    )
    cells, final = run_blocks(
        queries,
        key_float,
        value_float,
        input_gate,
        log_forget,
        documents,
        (before[0], before[1], before[2], before[4]),
    )
    gated = (cells.reshape(tokens, -1) * jax.nn.sigmoid(output_gate.astype(jnp.float32))).astype(
        jnp.bfloat16
    )
    mine = lax.all_to_all(gated, "tp", split_axis=0, concat_axis=1, tiled=True)
    projected = jnp.dot(
        mine,
        lax.all_gather(out_weight, "tp", axis=0, tiled=True),
        preferred_element_type=jnp.float32,
    )
    stream = residual.astype(jnp.float32) + projected
    normed = stream * lax.rsqrt(jnp.mean(stream * stream, axis=1, keepdims=True) + norm_eps)
    normed = (normed * norm_gain.astype(jnp.float32)).astype(jnp.bfloat16)
    rows_all = lax.all_gather(normed, "tp", axis=0, tiled=True)
    gate_act = jnp.dot(rows_all, whole_gate, preferred_element_type=jnp.float32)
    up_act = jnp.dot(rows_all, whole_up, preferred_element_type=jnp.float32)
    hidden = (jax.nn.silu(gate_act) * up_act).astype(jnp.bfloat16)
    partial_sum = jnp.dot(hidden, whole_down, preferred_element_type=jnp.float32)
    down = lax.psum_scatter(
        partial_sum.astype(jnp.bfloat16), "tp", scatter_dimension=0, tiled=True
    ).astype(jnp.float32)
    return (stream + 0.5 * down).astype(jnp.bfloat16)


def solution(mesh):
    torus = Mesh(mesh.devices.reshape(4, 4, 2, mesh.shape["tp"]), ("sp_0", "sp_1", "sp_2", "tp"))
    in_specs = (
        P(SP, "tp"),
        P(SP, "tp"),
        P(SP, "tp"),
        P("tp", SP),
        P("tp", SP),
        P(SP, "tp"),
        P(SP),
        P(SP_TP, None),
        P("tp", None),
        P(),
        P(SP, "tp"),
        P(SP, "tp"),
        P("tp", SP),
    )
    out_specs = P(SP_TP, None)
    return jax.shard_map(body, mesh=torus, in_specs=in_specs, out_specs=out_specs, check_vma=False)
```

profile of v0, /device:TPU:1, one launch (start us, length us, event | category | flops | bytes accessed | tf_op | source)
XLA Modules:
  0.0 448.9 jit_solution(14347902271754953552)
XLA Ops:
  10.0 1.9 slice_dynamic-update-slice_fusion
  11.9 1.3 broadcast_compare_fusion
  16.7 1.4 fusion.34
  18.0 1.7 fusion.32
  19.8 3.2 all-gather.3
  23.6 1.8 all-reduce.6
  31.0 11.8 %all-gather.4 = f32[4,260,128]{2,1,0:T(8,128)S(1)} all-gather(f32[1,260,128]{2,1,0:T(8,128)S(1)} %maximum_bitcast_fusion.1), channel_id=3, replica_groups=mesh['sp_0'=4,'sp_1'=4,'sp_2'=2,'tp'=4] {'sp_1'}, dimensions={0}, use_global_device_ids=true | all-gather | bytes 665600 | tf_op jit(solution)/shard_map/all_gather | solution.py:41
  45.5 6.5 %all-reduce.7 = s32[4]{0:T(128)S(1)} all-reduce(s32[4]{0:T(128)S(1)} %dynamic-update-slice.1), channel_id=1, replica_groups=mesh['sp_0'=4,'sp_1'=4,'sp_2'=2,'tp'=4] {'sp_1'}, use_global_device_ids=true, to_apply=%add.7 | all-reduce | flops 4 | bytes 32
  61.6 11.7 %all-gather.5 = f32[4,260,128]{2,1,0:T(8,128)S(1)} all-gather(f32[1,260,128]{2,1,0:T(8,128)S(1)} %maximum_bitcast_fusion.2), channel_id=4, replica_groups=mesh['sp_0'=4,'sp_1'=4,'sp_2'=2,'tp'=4] {'sp_0'}, dimensions={0}, use_global_device_ids=true | all-gather | bytes 665600 | tf_op jit(solution)/shard_map/all_gather | solution.py:41
  74.2 1.5 reshape.2044
  77.6 7.2 %all-reduce.8 = s32[4]{0:T(128)S(1)} all-reduce(s32[4]{0:T(128)S(1)} %dynamic-update-slice.2), channel_id=1, replica_groups=mesh['sp_0'=4,'sp_1'=4,'sp_2'=2,'tp'=4] {'sp_0'}, use_global_device_ids=true, to_apply=%add.8 | all-reduce | flops 4 | bytes 32
  94.1 1.5 reshape.2046
  95.9 1.8 add_select_fusion.3
  97.7 112.4 %while.18 = (s32[]{:T(128)}, f32[2,128,128]{2,1,0:T(8,128)S(1)}, f32[2,128]{1,0:T(2,128)S(1)}, f32[2]{0:T(128)S(1)}, s32[]{:T(128)}, /*index=5*/f32[8,128,2,128]...) while((s32[]{:T(128)}, f32[2,128,128]{2,1,0:T(8,128)S(1)}, ...), condition=%wide.region_8.9_spmd, body=%wide.region_3.8_spmd.sunk | while | flops 202756624 | bytes 3499011 | solution.py:136
  106.4 4.7 %dynamic_update_slice.5 = f32[8,128,2,128]{1,0,3,2:T(8,128)} dynamic-update-slice(f32[8,128,2,128]{1,0,3,2:T(8,128)} %get-tuple-element.360, f32[1,128,2,128]{1,0,3,2:T(1,128)S(1)} %copy.134, s32[]{:T(128)S(6)} %copy.145, s32[]{:T(128)} %constant.31.clone.1..sunk, s32[]{:T(128)} %constant.31.clone.1..sunk, s32[]{:T(128)} %constant.31.clone.1..sunk) | dynamic-update-slice | bytes 262148 | tf_op jit(solution)/shard_map/while/body/jit(dynamic_update_index_in_dim)/dynamic_update_slice | solution.py:136
  120.5 4.7 %dynamic_update_slice.5 = f32[8,128,2,128]{1,0,3,2:T(8,128)} dynamic-update-slice(f32[8,128,2,128]{1,0,3,2:T(8,128)} %get-tuple-element.360, f32[1,128,2,128]{1,0,3,2:T(1,128)S(1)} %copy.134, s32[]{:T(128)S(6)} %copy.145, s32[]{:T(128)} %constant.31.clone.1..sunk, s32[]{:T(128)} %constant.31.clone.1..sunk, s32[]{:T(128)} %constant.31.clone.1..sunk) | dynamic-update-slice | bytes 262148 | tf_op jit(solution)/shard_map/while/body/jit(dynamic_update_index_in_dim)/dynamic_update_slice | solution.py:136
  134.5 4.7 %dynamic_update_slice.5 = f32[8,128,2,128]{1,0,3,2:T(8,128)} dynamic-update-slice(f32[8,128,2,128]{1,0,3,2:T(8,128)} %get-tuple-element.360, f32[1,128,2,128]{1,0,3,2:T(1,128)S(1)} %copy.134, s32[]{:T(128)S(6)} %copy.145, s32[]{:T(128)} %constant.31.clone.1..sunk, s32[]{:T(128)} %constant.31.clone.1..sunk, s32[]{:T(128)} %constant.31.clone.1..sunk) | dynamic-update-slice | bytes 262148 | tf_op jit(solution)/shard_map/while/body/jit(dynamic_update_index_in_dim)/dynamic_update_slice | solution.py:136
  148.6 4.7 %dynamic_update_slice.5 = f32[8,128,2,128]{1,0,3,2:T(8,128)} dynamic-update-slice(f32[8,128,2,128]{1,0,3,2:T(8,128)} %get-tuple-element.360, f32[1,128,2,128]{1,0,3,2:T(1,128)S(1)} %copy.134, s32[]{:T(128)S(6)} %copy.145, s32[]{:T(128)} %constant.31.clone.1..sunk, s32[]{:T(128)} %constant.31.clone.1..sunk, s32[]{:T(128)} %constant.31.clone.1..sunk) | dynamic-update-slice | bytes 262148 | tf_op jit(solution)/shard_map/while/body/jit(dynamic_update_index_in_dim)/dynamic_update_slice | solution.py:136
  162.6 4.7 %dynamic_update_slice.5 = f32[8,128,2,128]{1,0,3,2:T(8,128)} dynamic-update-slice(f32[8,128,2,128]{1,0,3,2:T(8,128)} %get-tuple-element.360, f32[1,128,2,128]{1,0,3,2:T(1,128)S(1)} %copy.134, s32[]{:T(128)S(6)} %copy.145, s32[]{:T(128)} %constant.31.clone.1..sunk, s32[]{:T(128)} %constant.31.clone.1..sunk, s32[]{:T(128)} %constant.31.clone.1..sunk) | dynamic-update-slice | bytes 262148 | tf_op jit(solution)/shard_map/while/body/jit(dynamic_update_index_in_dim)/dynamic_update_slice | solution.py:136
  176.6 4.7 %dynamic_update_slice.5 = f32[8,128,2,128]{1,0,3,2:T(8,128)} dynamic-update-slice(f32[8,128,2,128]{1,0,3,2:T(8,128)} %get-tuple-element.360, f32[1,128,2,128]{1,0,3,2:T(1,128)S(1)} %copy.134, s32[]{:T(128)S(6)} %copy.145, s32[]{:T(128)} %constant.31.clone.1..sunk, s32[]{:T(128)} %constant.31.clone.1..sunk, s32[]{:T(128)} %constant.31.clone.1..sunk) | dynamic-update-slice | bytes 262148 | tf_op jit(solution)/shard_map/while/body/jit(dynamic_update_index_in_dim)/dynamic_update_slice | solution.py:136
  190.7 4.7 %dynamic_update_slice.5 = f32[8,128,2,128]{1,0,3,2:T(8,128)} dynamic-update-slice(f32[8,128,2,128]{1,0,3,2:T(8,128)} %get-tuple-element.360, f32[1,128,2,128]{1,0,3,2:T(1,128)S(1)} %copy.134, s32[]{:T(128)S(6)} %copy.145, s32[]{:T(128)} %constant.31.clone.1..sunk, s32[]{:T(128)} %constant.31.clone.1..sunk, s32[]{:T(128)} %constant.31.clone.1..sunk) | dynamic-update-slice | bytes 262148 | tf_op jit(solution)/shard_map/while/body/jit(dynamic_update_index_in_dim)/dynamic_update_slice | solution.py:136
  204.7 4.7 %dynamic_update_slice.5 = f32[8,128,2,128]{1,0,3,2:T(8,128)} dynamic-update-slice(f32[8,128,2,128]{1,0,3,2:T(8,128)} %get-tuple-element.360, f32[1,128,2,128]{1,0,3,2:T(1,128)S(1)} %copy.134, s32[]{:T(128)S(6)} %copy.145, s32[]{:T(128)} %constant.31.clone.1..sunk, s32[]{:T(128)} %constant.31.clone.1..sunk, s32[]{:T(128)} %constant.31.clone.1..sunk) | dynamic-update-slice | bytes 262148 | tf_op jit(solution)/shard_map/while/body/jit(dynamic_update_index_in_dim)/dynamic_update_slice | solution.py:136
  210.4 1.6 fusion.31
  212.8 3.7 all-to-all-start
  216.5 6.9 %all-to-all-done = bf16[4,256,256]{1,2,0:T(8,128)(2,1)S(1)} async-done(((bf16[4,256,256]{1,2,0:T(8,128)(2,1)}), bf16[4,256,256]{1,2,0:T(8,128)(2,1)S(1)}, u32[]{:S(2)}, u32[]{:S(2)}) %all-to-all-start) | async-done | bytes 524320 | tf_op jit(solution)/shard_map/all_to_all | solution.py:217
  223.4 3.9 multiply_reduce_fusion
  229.8 52.7 %all-gather.12.cloned.1.call-done = bf16[1024,2048]{1,0:T(8,128)(2,1)} async-done(((bf16[256,2048]{1,0:T(8,128)(2,1)}), bf16[1024,2048]{1,0:T(8,128)(2,1)}) %all-gather.12.cloned.1.call-update) | async-done | bytes 4194320 | tf_op jit(solution)/shard_map/all_gather | solution.py:226
  282.5 77.2 %all-gather.14.cloned.1.call-done = bf16[2048,4224]{1,0:T(8,128)(2,1)} async-done(((bf16[64,4224]{1,0:T(8,128)(2,1)}), bf16[2048,4224]{1,0:T(8,128)(2,1)}) %all-gather.14.cloned.1.call-update) | async-done | bytes 17301520 | tf_op jit(solution)/shard_map/all_gather | solution.py:19
  359.6 11.7 %fusion.21 = f32[1024,1408]{1,0:T(8,128)} fusion(bf16[1024,2048]{1,0:T(8,128)(2,1)} %all-gather.12.cloned.1.call-done, bf16[2048,4224]{1,0:T(8,128)(2,1)} %all-gather.14.cloned.1.call-done), kind=kOutput, calls=%fused_computation.48 | convolution fusion | flops 5905580032 | bytes 15728640 | tf_op jit(solution)/shard_map/dot_general | solution.py:227
  371.3 22.7 %fusion.25 = bf16[1024,2048]{1,0:T(8,128)(2,1)} fusion(bf16[2048,4224]{1,0:T(8,128)(2,1)} %all-gather.14.cloned.1.call-done, f32[1024,1408]{1,0:T(8,128)} %fusion.21, bf16[1024,2048]{1,0:T(8,128)(2,1)} %all-gather.12.cloned.1.call-done), kind=kOutput, calls=%fused_computation.51 | convolution fusion | flops 11821907968 | bytes 25690112 | tf_op jit(solution)/shard_map/dot_general | solution.py:230
  394.0 45.9 %reduce-scatter.2.cloned.1.call-done = bf16[256,2048]{1,0:T(8,128)(2,1)} async-done(((bf16[1024,2048]{1,0:T(8,128)(2,1)}), bf16[256,2048]{1,0:T(8,128)(2,1)}) %reduce-scatter.2.cloned.1.call-update) | async-done | bytes 1048592 | tf_op jit(solution)/shard_map/reduce_scatter | solution.py:231
  439.9 2.5 add_convert_fusion
  (295 shorter events, 85.3 us)
Async XLA Ops:
  6.5 37.1 %copy-start.9 = (u32[128]{0:T(128)S(1)}, u32[128]{0:T(128)}, u32[]{:S(2)}) copy-start(u32[128]{0:T(128)} %constant.104) | copy-start | bytes 1540
  6.5 38.5 %copy-start.1 = (bf16[1024,256]{1,0:T(8,128)(2,1)S(1)}, bf16[1024,256]{1,0:T(8,128)(2,1)}, u32[]{:S(2)}) copy-start(bf16[1024,256]{1,0:T(8,128)(2,1)} %param.17) | copy-start | bytes 1572868
  6.5 216.9 %all-gather.10.cloned.1.call-start = ((), (), s32[]{:S(2)}) async-start(), calls=%async_computation.2 | async-start | bytes 5242880 | tf_op jit(solution)/shard_map/all_gather | solution.py:220
  19.7 54.4 %copy-start = (bf16[1024,256]{1,0:T(8,128)(2,1)S(1)}, bf16[1024,256]{1,0:T(8,128)(2,1)}, u32[]{:S(2)}) copy-start(bf16[1024,256]{1,0:T(8,128)(2,1)} %param.16) | copy-start | bytes 1572868
  30.2 0.5 copy-start.7
  60.6 0.6 copy-start.8
  97.7 112.4 %copy-start.2 = (bf16[1024,256]{1,0:T(8,128)(2,1)S(1)}, bf16[1024,256]{1,0:T(8,128)(2,1)}, u32[]{:S(2)}) copy-start(bf16[1024,256]{1,0:T(8,128)(2,1)} %param.20) | copy-start | bytes 1572868
  210.1 6.4 %copy-start.6 = (bf16[2048]{0:T(1024)(128)(2,1)S(1)}, bf16[2048]{0:T(1024)(128)(2,1)}, u32[]{:S(2)}) copy-start(bf16[2048]{0:T(1024)(128)(2,1)} %param.24) | copy-start | bytes 12292
  212.8 10.7 %all-to-all-start = ((bf16[4,256,256]{1,2,0:T(8,128)(2,1)}), bf16[4,256,256]{1,2,0:T(8,128)(2,1)S(1)}, u32[]{:S(2)}, u32[]{:S(2)}) async-start(bf16[4,256,256]{1,2,0:T(8,128)(2,1)} %bitcast.516), calls=%async_computation | async-start | bytes 1048576 | tf_op jit(solution)/shard_map/all_to_all | solution.py:217
  216.5 66.0 %all-gather.12.cloned.1.call-start = ((), (), s32[]{:S(2)}) async-start(), calls=%async_computation.3 | async-start | bytes 5242880 | tf_op jit(solution)/shard_map/all_gather | solution.py:226
  227.3 1.3 copy-start.3
  227.3 1.3 copy-start.4
  227.3 1.3 copy-start.5
  228.6 131.1 %all-gather.14.cloned.1.call-start = ((), (), s32[]{:S(2)}) async-start(), calls=%async_computation.4 | async-start | bytes 17842176 | tf_op jit(solution)/shard_map/all_gather | solution.py:19
  229.5 210.4 %reduce-scatter.2.cloned.1.call-start = ((), (), s32[]{:S(2)}) async-start(), calls=%async_computation.5 | async-start | bytes 5242880 | tf_op jit(solution)/shard_map/reduce_scatter | solution.py:231
Sparse Core Ops, SparseCore 0:
  9.0 51.1 all-gather.9
  228.7 53.7 all-gather.11
  284.7 74.8 all-gather.13
  394.2 45.7 reduce-scatter.1
where the time goes:
time: 451 us; the launch traced here: 449 us
  waiting for transfers between devices  183 us (41%)
  local copies, waits for them, and re-layouts  78.3 us (17%)
  matrix products  58.1 us (13%)
  blocking collectives  42.2 us (9%)
  other arithmetic  39.2 us (9%)
  between operations  32.8 us (7%)
  loops' own time  10.8 us (2%)
    all_gather x1, waiting for transfers between devices, gather_turned(): lax.all_gather(both, axis, axis=0, tiled=True)  77.2 us
    all_gather x1, waiting for transfers between devices, body(): rows_all = lax.all_gather(normed, 'tp', axis=0, tiled=True)  52.7 us
    reduce_scatter x1, waiting for transfers between devices, body(): lax.psum_scatter(partial_sum.astype(jnp.bfloat16), 'tp', scatter_dimensio...  45.9 us
    dynamic_update_slice x16, local copies, waits for them, and re-layouts, run_blocks(): final, outputs = lax.scan(block_step, start_state, inputs)  38.7 us
    all_gather x3, blocking collectives, all_in_one(): both, at, found = (lax.all_gather(jnp.concatenate(lines), axis), 0, {})  26.6 us
    dot_general x1, matrix products, body(): jnp.dot(hidden, whole_down, preferred_element_type=jnp.float32)  22.7 us
    unnamed x3, blocking collectives  15.6 us
    dynamic_slice x16, local copies, waits for them, and re-layouts, run_blocks(): final, outputs = lax.scan(block_step, start_state, inputs)  14.8 us
  transfers between devices with their start and end apart: 5, of which 4 were waited for; matrix products, arithmetic and copies ran while one was open for 30% of the time, Pallas kernels for 0%

commit v1 on v0

--- a/solution.py
+++ b/solution.py
@@ -223,7 +223,19 @@
     stream = residual.astype(jnp.float32) + projected
     normed = stream * lax.rsqrt(jnp.mean(stream * stream, axis=1, keepdims=True) + norm_eps)
     normed = (normed * norm_gain.astype(jnp.float32)).astype(jnp.bfloat16)
-    rows_all = lax.all_gather(normed, "tp", axis=0, tiled=True)
+
+    def remake_records(matrix):
+        return jnp.concatenate(
+            lax.all_to_all(
+                jnp.stack([matrix for _ in range(lax.axis_size("tp"))], axis=0),
+                axis_name="tp",
+                split_axis=0,
+                concat_axis=0,
+            ),
+            0,
+        )
+
+    rows_all = remake_records(normed)
     gate_act = jnp.dot(rows_all, whole_gate, preferred_element_type=jnp.float32)
     up_act = jnp.dot(rows_all, whole_up, preferred_element_type=jnp.float32)
     hidden = (jax.nn.silu(gate_act) * up_act).astype(jnp.bfloat16)

time: 451 us -> 372 us (0.82)
  waiting for transfers between devices: 183 us -> 60.4 us
  blocking collectives: 42.2 us -> 85.8 us
    all_gather x1, waiting for transfers between devices: 77.2 us -> 0.01 us  [gather_turned(): lax.all_gather(both, axis, axis=0, tiled=True)]
    all_gather x1 -> x0, waiting for transfers between devices: 52.7 us -> none  [body(): rows_all = lax.all_gather(normed, 'tp', axis=0, tiled=True)]
    all_to_all x0 -> x1, blocking collectives: none -> 43.1 us  [remake_records(): lax.all_to_all(jnp.stack([matrix for _ in range(lax.axis_size('tp'))], ax...]
    reduce_scatter x1, waiting for transfers between devices: 45.9 us -> 52.8 us  [body(): lax.psum_scatter(partial_sum.astype(jnp.bfloat16), 'tp', scatter_dimensio...]
  transfers between devices with their start and end apart: 5 -> 4, of which waited for: 4 -> 2; matrix products, arithmetic and copies ran while one was open for 30% -> 38% of each run, Pallas kernels for 0% -> 0%
where the time goes in v1:
time: 372 us; the launch traced here: 369 us
  blocking collectives  85.8 us (23%)
  local copies, waits for them, and re-layouts  79.2 us (21%)
  waiting for transfers between devices  60.4 us (16%)
  matrix products  56 us (15%)
  other arithmetic  40.4 us (11%)
  between operations  32.5 us (9%)
  loops' own time  11 us (3%)
  starting transfers between devices  3.77 us (1%)
    reduce_scatter x1, waiting for transfers between devices, body(): lax.psum_scatter(partial_sum.astype(jnp.bfloat16), 'tp', scatter_dimensio...  52.8 us
    all_to_all x1, blocking collectives, remake_records(): lax.all_to_all(jnp.stack([matrix for _ in range(lax.axis_size('tp'))], ax...  43.1 us
    dynamic_update_slice x16, local copies, waits for them, and re-layouts, run_blocks(): final, outputs = lax.scan(block_step, start_state, inputs)  38.8 us
    all_gather x3, blocking collectives, all_in_one(): both, at, found = (lax.all_gather(jnp.concatenate(lines), axis), 0, {})  26.5 us
    dot_general x1, matrix products, body(): jnp.dot(hidden, whole_down, preferred_element_type=jnp.float32)  22.6 us
    unnamed x3, blocking collectives  16.2 us
    dynamic_slice x16, local copies, waits for them, and re-layouts, run_blocks(): final, outputs = lax.scan(block_step, start_state, inputs)  14.9 us
    dot_general x1, matrix products, body(): gate_act = jnp.dot(rows_all, whole_gate, preferred_element_type=jnp.float32)  11.7 us
  transfers between devices with their start and end apart: 4, of which 2 were waited for; matrix products, arithmetic and copies ran while one was open for 38% of the time, Pallas kernels for 0%

profile of v1, /device:TPU:1, one launch (start us, length us, event | category | flops | bytes accessed | tf_op | source)
XLA Modules:
  0.0 369.1 jit_solution(16203192262797785684)
XLA Ops:
  7.3 1.9 pad_maximum_fusion
  12.0 2.0 slice_dynamic-update-slice_fusion
  14.0 1.3 broadcast_compare_fusion
  17.5 1.2 copy.56
  19.8 3.0 all-gather.3
  23.5 1.8 all-reduce.6
  30.1 11.8 %all-gather.4 = f32[4,260,128]{2,1,0:T(8,128)S(1)} all-gather(f32[1,260,128]{2,1,0:T(8,128)S(1)} %maximum_bitcast_fusion.1), channel_id=3, replica_groups=mesh['sp_0'=4,'sp_1'=4,'sp_2'=2,'tp'=4] {'sp_1'}, dimensions={0}, use_global_device_ids=true | all-gather | bytes 665600 | tf_op jit(solution)/shard_map/all_gather | solution.py:41
  44.6 6.5 %all-reduce.7 = s32[4]{0:T(128)S(1)} all-reduce(s32[4]{0:T(128)S(1)} %dynamic-update-slice.1), channel_id=1, replica_groups=mesh['sp_0'=4,'sp_1'=4,'sp_2'=2,'tp'=4] {'sp_1'}, use_global_device_ids=true, to_apply=%add.7 | all-reduce | flops 4 | bytes 32
  59.9 11.7 %all-gather.5 = f32[4,260,128]{2,1,0:T(8,128)S(1)} all-gather(f32[1,260,128]{2,1,0:T(8,128)S(1)} %maximum_bitcast_fusion.2), channel_id=4, replica_groups=mesh['sp_0'=4,'sp_1'=4,'sp_2'=2,'tp'=4] {'sp_0'}, dimensions={0}, use_global_device_ids=true | all-gather | bytes 665600 | tf_op jit(solution)/shard_map/all_gather | solution.py:41
  72.5 1.5 reshape.2050
  75.4 7.8 %all-reduce.8 = s32[4]{0:T(128)S(1)} all-reduce(s32[4]{0:T(128)S(1)} %dynamic-update-slice.2), channel_id=1, replica_groups=mesh['sp_0'=4,'sp_1'=4,'sp_2'=2,'tp'=4] {'sp_0'}, use_global_device_ids=true, to_apply=%add.8 | all-reduce | flops 4 | bytes 32
  91.5 2.0 copy.45
  94.7 1.5 reshape.2052
  97.2 2.0 add_select_fusion.3
  99.3 112.8 %while.18 = (s32[]{:T(128)}, f32[2,128,128]{2,1,0:T(8,128)S(1)}, f32[2,128]{1,0:T(2,128)S(1)}, f32[2]{0:T(128)S(1)}, s32[]{:T(128)}, /*index=5*/f32[8,128,2,128]...) while((s32[]{:T(128)}, f32[2,128,128]{2,1,0:T(8,128)S(1)}, ...), condition=%wide.region_8.9_spmd, body=%wide.region_3.8_spmd.sunk | while | flops 202756624 | bytes 3499011 | solution.py:136
  108.0 4.8 %dynamic_update_slice.5 = f32[8,128,2,128]{1,0,3,2:T(8,128)} dynamic-update-slice(f32[8,128,2,128]{1,0,3,2:T(8,128)} %get-tuple-element.360, f32[1,128,2,128]{1,0,3,2:T(1,128)S(1)} %copy.134, s32[]{:T(128)S(6)} %copy.145, s32[]{:T(128)} %constant.31.clone.1..sunk, s32[]{:T(128)} %constant.31.clone.1..sunk, s32[]{:T(128)} %constant.31.clone.1..sunk) | dynamic-update-slice | bytes 262148 | tf_op jit(solution)/shard_map/while/body/jit(dynamic_update_index_in_dim)/dynamic_update_slice | solution.py:136
  122.1 4.8 %dynamic_update_slice.5 = f32[8,128,2,128]{1,0,3,2:T(8,128)} dynamic-update-slice(f32[8,128,2,128]{1,0,3,2:T(8,128)} %get-tuple-element.360, f32[1,128,2,128]{1,0,3,2:T(1,128)S(1)} %copy.134, s32[]{:T(128)S(6)} %copy.145, s32[]{:T(128)} %constant.31.clone.1..sunk, s32[]{:T(128)} %constant.31.clone.1..sunk, s32[]{:T(128)} %constant.31.clone.1..sunk) | dynamic-update-slice | bytes 262148 | tf_op jit(solution)/shard_map/while/body/jit(dynamic_update_index_in_dim)/dynamic_update_slice | solution.py:136
  136.2 4.7 %dynamic_update_slice.5 = f32[8,128,2,128]{1,0,3,2:T(8,128)} dynamic-update-slice(f32[8,128,2,128]{1,0,3,2:T(8,128)} %get-tuple-element.360, f32[1,128,2,128]{1,0,3,2:T(1,128)S(1)} %copy.134, s32[]{:T(128)S(6)} %copy.145, s32[]{:T(128)} %constant.31.clone.1..sunk, s32[]{:T(128)} %constant.31.clone.1..sunk, s32[]{:T(128)} %constant.31.clone.1..sunk) | dynamic-update-slice | bytes 262148 | tf_op jit(solution)/shard_map/while/body/jit(dynamic_update_index_in_dim)/dynamic_update_slice | solution.py:136
  150.3 4.7 %dynamic_update_slice.5 = f32[8,128,2,128]{1,0,3,2:T(8,128)} dynamic-update-slice(f32[8,128,2,128]{1,0,3,2:T(8,128)} %get-tuple-element.360, f32[1,128,2,128]{1,0,3,2:T(1,128)S(1)} %copy.134, s32[]{:T(128)S(6)} %copy.145, s32[]{:T(128)} %constant.31.clone.1..sunk, s32[]{:T(128)} %constant.31.clone.1..sunk, s32[]{:T(128)} %constant.31.clone.1..sunk) | dynamic-update-slice | bytes 262148 | tf_op jit(solution)/shard_map/while/body/jit(dynamic_update_index_in_dim)/dynamic_update_slice | solution.py:136
  164.4 4.7 %dynamic_update_slice.5 = f32[8,128,2,128]{1,0,3,2:T(8,128)} dynamic-update-slice(f32[8,128,2,128]{1,0,3,2:T(8,128)} %get-tuple-element.360, f32[1,128,2,128]{1,0,3,2:T(1,128)S(1)} %copy.134, s32[]{:T(128)S(6)} %copy.145, s32[]{:T(128)} %constant.31.clone.1..sunk, s32[]{:T(128)} %constant.31.clone.1..sunk, s32[]{:T(128)} %constant.31.clone.1..sunk) | dynamic-update-slice | bytes 262148 | tf_op jit(solution)/shard_map/while/body/jit(dynamic_update_index_in_dim)/dynamic_update_slice | solution.py:136
  178.5 4.7 %dynamic_update_slice.5 = f32[8,128,2,128]{1,0,3,2:T(8,128)} dynamic-update-slice(f32[8,128,2,128]{1,0,3,2:T(8,128)} %get-tuple-element.360, f32[1,128,2,128]{1,0,3,2:T(1,128)S(1)} %copy.134, s32[]{:T(128)S(6)} %copy.145, s32[]{:T(128)} %constant.31.clone.1..sunk, s32[]{:T(128)} %constant.31.clone.1..sunk, s32[]{:T(128)} %constant.31.clone.1..sunk) | dynamic-update-slice | bytes 262148 | tf_op jit(solution)/shard_map/while/body/jit(dynamic_update_index_in_dim)/dynamic_update_slice | solution.py:136
  192.6 4.7 %dynamic_update_slice.5 = f32[8,128,2,128]{1,0,3,2:T(8,128)} dynamic-update-slice(f32[8,128,2,128]{1,0,3,2:T(8,128)} %get-tuple-element.360, f32[1,128,2,128]{1,0,3,2:T(1,128)S(1)} %copy.134, s32[]{:T(128)S(6)} %copy.145, s32[]{:T(128)} %constant.31.clone.1..sunk, s32[]{:T(128)} %constant.31.clone.1..sunk, s32[]{:T(128)} %constant.31.clone.1..sunk) | dynamic-update-slice | bytes 262148 | tf_op jit(solution)/shard_map/while/body/jit(dynamic_update_index_in_dim)/dynamic_update_slice | solution.py:136
  206.7 4.7 %dynamic_update_slice.5 = f32[8,128,2,128]{1,0,3,2:T(8,128)} dynamic-update-slice(f32[8,128,2,128]{1,0,3,2:T(8,128)} %get-tuple-element.360, f32[1,128,2,128]{1,0,3,2:T(1,128)S(1)} %copy.134, s32[]{:T(128)S(6)} %copy.145, s32[]{:T(128)} %constant.31.clone.1..sunk, s32[]{:T(128)} %constant.31.clone.1..sunk, s32[]{:T(128)} %constant.31.clone.1..sunk) | dynamic-update-slice | bytes 262148 | tf_op jit(solution)/shard_map/while/body/jit(dynamic_update_index_in_dim)/dynamic_update_slice | solution.py:136
  212.1 1.6 fusion.31
  214.6 3.7 %all-to-all-start = ((bf16[4,256,256]{1,2,0:T(8,128)(2,1)}), bf16[4,256,256]{1,2,0:T(8,128)(2,1)S(1)}, u32[]{:S(2)}, u32[]{:S(2)}) async-start(bf16[4,256,256]{1,2,0:T(8,128)(2,1)} %bitcast.517), calls=%async_computation | async-start | bytes 1048576 | tf_op jit(solution)/shard_map/all_to_all | solution.py:217
  218.3 6.9 %all-to-all-done = bf16[4,256,256]{1,2,0:T(8,128)(2,1)S(1)} async-done(((bf16[4,256,256]{1,2,0:T(8,128)(2,1)}), bf16[4,256,256]{1,2,0:T(8,128)(2,1)S(1)}, u32[]{:S(2)}, u32[]{:S(2)}) %all-to-all-start) | async-done | bytes 524320 | tf_op jit(solution)/shard_map/all_to_all | solution.py:217
  225.2 3.9 %multiply_reduce_fusion = (f32[256]{0:T(256)S(1)}, f32[256,2048]{1,0:T(8,128)S(1)}) fusion(bf16[256,1024]{0,1:T(8,128)(2,1)S(1)} %bitcast.575, bf16[1024,2048]{1,0:T(8,128)(2,1)} %all-gather.9.cloned.1.call-done, bf16[256,2048]{1,0:T(8,128)(2,1)} %param.22), kind=kOutput, calls=%fused_computation.56 | convolution fusion | flops 1075838720 | bytes 7865344 | tf_op jit(solution)/shard_map/dot_general | solution.py:218
  229.9 43.1 %all_to_all.24 = bf16[4,256,2048]{2,1,0:T(8,128)(2,1)} all-to-all(bf16[4,256,2048]{2,1,0:T(8,128)(2,1)S(1)} %stack.2), channel_id=1, replica_groups=mesh['sp_0'=4,'sp_1'=4,'sp_2'=2,'tp'=4] {'tp'}, dimensions={0} | all-to-all | bytes 8388608 | tf_op jit(solution)/shard_map/all_to_all | solution.py:229
  273.0 11.7 %fusion.21 = f32[1024,1408]{1,0:T(8,128)} fusion(bf16[1024,2048]{1,0:T(8,128)(2,1)} %bitcast.572, bf16[2048,4224]{1,0:T(8,128)(2,1)} %all-gather.11.cloned.1.call-done), kind=kOutput, calls=%fused_computation.48 | convolution fusion | flops 5905580032 | bytes 15728640 | tf_op jit(solution)/shard_map/dot_general | solution.py:239
  284.6 22.6 %fusion.25 = bf16[1024,2048]{1,0:T(8,128)(2,1)} fusion(bf16[2048,4224]{1,0:T(8,128)(2,1)} %all-gather.11.cloned.1.call-done, f32[1024,1408]{1,0:T(8,128)} %fusion.21, bf16[1024,2048]{1,0:T(8,128)(2,1)} %bitcast.573), kind=kOutput, calls=%fused_computation.51 | convolution fusion | flops 11821907968 | bytes 25690112 | tf_op jit(solution)/shard_map/dot_general | solution.py:242
  307.3 52.8 %reduce-scatter.2.cloned.1.call-done = bf16[256,2048]{1,0:T(8,128)(2,1)} async-done(((bf16[1024,2048]{1,0:T(8,128)(2,1)}), bf16[256,2048]{1,0:T(8,128)(2,1)}) %reduce-scatter.2.cloned.1.call-update) | async-done | bytes 1048592 | tf_op jit(solution)/shard_map/reduce_scatter | solution.py:243
  360.1 2.5 add_convert_fusion
  (294 shorter events, 82.6 us)
Async XLA Ops:
  6.5 12.2 %copy-start = (bf16[1024,256]{1,0:T(8,128)(2,1)S(1)}, bf16[1024,256]{1,0:T(8,128)(2,1)}, u32[]{:S(2)}) copy-start(bf16[1024,256]{1,0:T(8,128)(2,1)} %param.16) | copy-start | bytes 1572868
  6.5 12.5 %copy-start.2 = (bf16[1024,256]{1,0:T(8,128)(2,1)S(1)}, bf16[1024,256]{1,0:T(8,128)(2,1)}, u32[]{:S(2)}) copy-start(bf16[1024,256]{1,0:T(8,128)(2,1)} %param.17) | copy-start | bytes 1572868
  6.5 218.7 %all-gather.9.cloned.1.call-start = ((), (), s32[]{:S(2)}) async-start(), calls=%async_computation.3 | async-start | bytes 5242880 | tf_op jit(solution)/shard_map/all_gather | solution.py:220
  7.3 265.7 %all-gather.11.cloned.1.call-start = ((), (), s32[]{:S(2)}) async-start(), calls=%async_computation.4 | async-start | bytes 17842176 | tf_op jit(solution)/shard_map/all_gather | solution.py:19
  9.2 33.5 %copy-start.9 = (u32[128]{0:T(128)S(1)}, u32[128]{0:T(128)}, u32[]{:S(2)}) copy-start(u32[128]{0:T(128)} %constant.104) | copy-start | bytes 1540
  29.9 44.1 %copy-start.8 = (u32[128]{0:T(128)S(1)}, u32[128]{0:T(128)}, u32[]{:S(2)}) copy-start(u32[128]{0:T(128)} %constant.109) | copy-start | bytes 1540
  71.6 19.9 %copy-start.1 = (f32[4,260,128]{2,1,0:T(8,128)}, f32[4,260,128]{2,1,0:T(8,128)S(1)}, u32[]{:S(2)}) copy-start(f32[4,260,128]{2,1,0:T(8,128)S(1)} %all-gather.5) | copy-start | bytes 1597444
  74.0 23.2 %copy-start.4 = (f32[1,256,128]{2,1,0:T(8,128)S(1)}, f32[1,256,128]{2,1,0:T(8,128)}, u32[]{:S(2)}) copy-start(f32[1,256,128]{2,1,0:T(8,128)} %get-tuple-element.171) | copy-start | bytes 393220
  74.0 23.2 %copy-start.5 = (f32[1,256,128]{2,1,0:T(8,128)S(1)}, f32[1,256,128]{2,1,0:T(8,128)}, u32[]{:S(2)}) copy-start(f32[1,256,128]{2,1,0:T(8,128)} %get-tuple-element.172) | copy-start | bytes 393220
  74.0 23.2 %copy-start.6 = (f32[1,256,128]{2,1,0:T(8,128)S(1)}, f32[1,256,128]{2,1,0:T(8,128)}, u32[]{:S(2)}) copy-start(f32[1,256,128]{2,1,0:T(8,128)} %get-tuple-element.173) | copy-start | bytes 393220
  99.3 112.9 %copy-start.3 = (bf16[1024,256]{0,1:T(8,128)(2,1)S(1)}, bf16[1024,256]{0,1:T(8,128)(2,1)}, u32[]{:S(2)}) copy-start(bf16[1024,256]{0,1:T(8,128)(2,1)} %copy.45) | copy-start | bytes 1572868
  212.1 6.2 %copy-start.7 = (bf16[2048]{0:T(1024)(128)(2,1)S(1)}, bf16[2048]{0:T(1024)(128)(2,1)}, u32[]{:S(2)}) copy-start(bf16[2048]{0:T(1024)(128)(2,1)} %param.24) | copy-start | bytes 12292
  214.6 10.7 %all-to-all-start = ((bf16[4,256,256]{1,2,0:T(8,128)(2,1)}), bf16[4,256,256]{1,2,0:T(8,128)(2,1)S(1)}, u32[]{:S(2)}, u32[]{:S(2)}) async-start(bf16[4,256,256]{1,2,0:T(8,128)(2,1)} %bitcast.517), calls=%async_computation | async-start | bytes 1048576 | tf_op jit(solution)/shard_map/all_to_all | solution.py:217
  218.3 141.8 %reduce-scatter.2.cloned.1.call-start = ((), (), s32[]{:S(2)}) async-start(), calls=%async_computation.5 | async-start | bytes 5242880 | tf_op jit(solution)/shard_map/reduce_scatter | solution.py:243
Sparse Core Ops, SparseCore 0:
  9.0 51.1 all-gather.8
  62.4 74.9 all-gather.10
  307.4 52.5 reduce-scatter.1
